TPU v7x, 32 devices: a whole 2x2x4 slice. The times are simulated.
32 devices in a mesh: grp: 2 (over y), ep: 8 (over z, x), tp: 2 (over core).
Axes of the slice: x: 2, y: 2, z: 4, core: 2. Of those that a mesh axis runs over, the one named last changes fastest.
Arguments:
- tokens: bfloat16 [1024, 2048], P(('grp', 'ep')), parts along dimension 0, may hold values from -6 to 6
- chosen: int32 [1, 16, 9], P(None, ('grp', 'ep')), parts along dimension 1, may hold values from -1 to 63, as said below
- route_weight: float32 [1, 16, 9], P(None, ('grp', 'ep')), parts along dimension 1, may hold values from 0.1 to 1
- expert_gate: bfloat16 [2048, 4096], P(None, ('ep', 'tp')), may hold values from -0.125 to 0.125
- expert_up: bfloat16 [2048, 4096], P(None, ('ep', 'tp')), may hold values from -0.125 to 0.125
- expert_down: bfloat16 [4096, 2048], P(('ep', 'tp')), may hold values from -0.09375 to 0.09375
- dense_gate: bfloat16 [2048, 512], P('ep', 'tp'), may hold values from -0.125 to 0.125
- dense_up: bfloat16 [2048, 512], P('ep', 'tp'), may hold values from -0.125 to 0.125
- dense_down: bfloat16 [512, 2048], P('tp', 'ep'), may hold values from -0.25 to 0.25
- branch_gate: float32 [2048], P('tp'), may hold values from -6 to 6
Outputs:
- mixed: bfloat16 [1024, 2048], P(('grp', 'ep'), 'tp'), parts along dimension 0
There are 2 independent parts, one for each index of `grp`. A program takes and returns all parts, laid end to end along the dimension named above; an argument that names none is the same for every part. Nothing has to cross between parts.
Inputs may be any that keep to these rules, and one draw needn't show every extreme that they name: chosen[e, s, k] is -1 or an index local to device s (token s * 64 + chosen[e, s, k] of the whole). In each (e, s) row the live entries come first and are distinct, the -1 entries follow. Each expert takes exactly 64 tokens in all, at most 9 from one device, and for every expert some device gives it exactly 9.
All inputs are finite; a program needn't handle non-finite values.
Results may differ from a plain program's by a relative error of at most 0.0085.
Values may be sent and summed in bfloat16 or wider, within the bound.
A program may use at most 64 MiB of HBM per device.

v0:
```python
import jax
import jax.numpy as jnp
from jax import lax
from jax.sharding import PartitionSpec as P


def swapped(block, axis, apart):
    count = lax.axis_size(axis)
    route = []
    for low in range(count):
        high = low | 1 << apart
        if high != low and high < count:
            route += [(low, high), (high, low)]
    return lax.ppermute(block, axis, route)


def expert_hidden(received, gate_cols, up_cols):
    flat_rows = received.reshape(-1, received.shape[-1])
    gate_act = jnp.dot(flat_rows, gate_cols, preferred_element_type=jnp.float32)
    up_act = jnp.dot(flat_rows, up_cols, preferred_element_type=jnp.float32)
    hidden = (jax.nn.silu(gate_act) * up_act).astype(jnp.bfloat16)
    return hidden.reshape(received.shape[0], received.shape[1], gate_cols.shape[1])


def join_pieces(mine, theirs, upper):
    return jnp.where(upper, jnp.concatenate([theirs, mine], 2), jnp.concatenate([mine, theirs], 2))


def local(
    tokens,
    chosen,
    route_weight,
    expert_gate,
    expert_up,
    expert_down,
    dense_gate,
    dense_up,
    dense_down,
    branch_gate,
):
    ep_count = lax.axis_size("ep")
    experts = chosen.shape[0]
    slots = chosen.shape[2]
    tok_local = tokens.shape[0]
    width = tokens.shape[1]
    picked = chosen[:, 0, :]
    filled = picked >= 0
    token_rows = jnp.take(tokens, jnp.maximum(picked, 0).reshape(-1), axis=0).reshape(
        experts, slots, width
    )
    token_rows = jnp.where(filled[:, :, None], token_rows, jnp.zeros((), jnp.bfloat16))
    send_width = token_rows.shape[2]
    piece = send_width // 8
    split_rows = jnp.transpose(token_rows.reshape(experts, slots, 8, piece), (0, 2, 1, 3)).reshape(
        ep_count, slots, piece
    )
    own_piece = lax.all_to_all(split_rows, "ep", split_axis=0, concat_axis=0, tiled=True)
    member = lax.axis_index("ep") % 8
    current = own_piece[:, :, None, :]
    partner = swapped(current, "ep", 0)
    current = join_pieces(current, partner, member % 2 == 1)
    partner = swapped(current, "ep", 1)
    current = join_pieces(current, partner, member // 2 % 2 == 1)
    partner = swapped(current, "ep", 2)
    current = join_pieces(current, partner, member // 4 == 1)
    received = current.reshape(ep_count, slots, send_width)
    hidden = expert_hidden(received, gate_cols=expert_gate, up_cols=expert_up)
    flat_hidden = hidden.reshape(ep_count * slots, -1)
    shard_rows = expert_down
    member_sums = lax.psum_scatter(
        lax.dot_general(
            shard_rows, flat_hidden, (((0,), (1,)), ((), ())), preferred_element_type=jnp.float32
        ).astype(jnp.bfloat16),
        "tp",
        scatter_dimension=0,
        tiled=True,
    )
    returned = lax.all_to_all(member_sums, "ep", split_axis=1, concat_axis=1, tiled=True)
    summed = returned.astype(jnp.float32).reshape(width // 2, experts, 8, slots).sum(axis=2)
    positions = lax.broadcasted_iota(jnp.int32, (experts, slots, tok_local), 2)
    weights_table = jnp.where(picked[:, :, None] == positions, route_weight[:, 0, :, None], 0.0)
    combined = jnp.einsum("fek,ekt->tf", summed, weights_table, precision=lax.Precision.HIGHEST)
    shard_rows = (
        lax.all_gather(dense_gate, "ep", axis=0, tiled=True),
        lax.all_gather(dense_up, "ep", axis=0, tiled=True),
    )
    gate_dense = jnp.dot(tokens, shard_rows[0], preferred_element_type=jnp.float32)
    up_dense = jnp.dot(tokens, shard_rows[1], preferred_element_type=jnp.float32)
    dense_hidden = (jax.nn.silu(gate_dense) * up_dense).astype(jnp.bfloat16)
    dense_terms = jnp.dot(
        dense_hidden,
        lax.all_gather(dense_down, "ep", axis=1, tiled=True),
        preferred_element_type=jnp.float32,
    )
    dense_sum = lax.psum_scatter(
        dense_terms.astype(jnp.bfloat16), "tp", scatter_dimension=1, tiled=True
    ).astype(jnp.float32)
    return (combined + jax.nn.sigmoid(branch_gate)[None, :] * dense_sum).astype(jnp.bfloat16)


def solution(mesh):
    return jax.shard_map(
        local,
        mesh=mesh,
        in_specs=(
            P(("grp", "ep"), None),
            P(None, ("grp", "ep"), None),
            P(None, ("grp", "ep"), None),
            P(None, ("ep", "tp")),
            P(None, ("ep", "tp")),
            P(("ep", "tp"), None),
            P("ep", "tp"),
            P("ep", "tp"),
            P("tp", "ep"),
            P("tp"),
        ),
        out_specs=P(("grp", "ep"), "tp"),
        check_vma=False,
    )
```

profile of v0, /device:TPU:0, one launch (start us, length us, event | category | flops | bytes accessed | tf_op | source)
XLA Modules:
  0.0 162.1 jit_solution(17605187083843992932)
XLA Ops:
  7.4 0.0 copy-start
  7.4 0.0 copy-start.1
  7.4 0.0 all-gather.4.cloned.1.call-start
  7.4 0.7 all-gather.4.cloned.1.call-update
  8.1 0.0 all-gather.6.cloned.1.call-start
  8.1 0.7 all-gather.6.cloned.1.call-update
  8.8 0.0 copy-start.4
  8.9 0.0 all-gather.8.cloned.1.call-start
  8.9 0.7 all-gather.8.cloned.1.call-update
  9.6 0.0 reduce-scatter.3.cloned.1.call-start
  9.6 0.0 copy-done.4
  9.7 0.0 copy-done.1
  9.7 0.6 gather_fusion
  10.3 0.1 fusion.10
  10.4 14.1 %all_to_all.14 = bf16[8,9,256]{2,1,0:T(8,128)(2,1)S(1)} all-to-all(bf16[8,9,256]{2,1,0:T(8,128)(2,1)S(1)} %fusion.10), channel_id=1, replica_groups=mesh['grp'=2,'ep'=8,'tp'=2] {'ep'}, dimensions={0} | all-to-all | bytes 73728 | tf_op jit(solution)/shard_map/all_to_all | solution.py:57
  24.5 0.4 collective-permute-start
  24.9 3.7 %collective-permute-done = bf16[8,9,1,256]{3,0,2,1:T(8,128)(2,1)S(1)} collective-permute-done((bf16[8,9,1,256]{3,0,2,1:T(8,128)(2,1)S(1)}, bf16[8,9,1,256]{3,0,2,1:T(8,128)(2,1)S(1)}, u32[]{:S(2)}, u32[]{:S(2)}) %collective-permute-start) | collective-permute-done | bytes 36896 | tf_op jit(solution)/shard_map/ppermute | solution.py:14
  28.5 0.2 collective-permute-start.1
  28.7 0.0 copy-start.2
  28.7 4.7 %collective-permute-done.1 = bf16[8,9,2,256]{3,0,2,1:T(8,128)(2,1)S(1)} collective-permute-done((bf16[8,9,2,256]{3,0,2,1:T(8,128)(2,1)S(1)}, bf16[8,9,2,256]{3,0,2,1:T(8,128)(2,1)S(1)}, u32[]{:S(2)}, u32[]{:S(2)}) %collective-permute-start.1) | collective-permute-done | bytes 73760 | tf_op jit(solution)/shard_map/ppermute | solution.py:14
  33.5 0.5 collective-permute-start.2
  34.0 6.7 %collective-permute-done.2 = bf16[8,9,4,256]{3,0,2,1:T(8,128)(2,1)S(1)} collective-permute-done((bf16[8,9,4,256]{3,0,2,1:T(8,128)(2,1)S(1)}, bf16[8,9,4,256]{3,0,2,1:T(8,128)(2,1)S(1)}, u32[]{:S(2)}, u32[]{:S(2)}) %collective-permute-start.2) | collective-permute-done | bytes 147488 | tf_op jit(solution)/shard_map/ppermute | solution.py:14
  40.7 0.1 copy.15
  40.8 0.1 copy.17
  40.9 0.0 copy-done.2
  40.9 0.3 fusion.25
  41.2 0.0 copy-done
  41.2 2.7 %fusion = bf16[2048,72]{0,1:T(8,128)(2,1)} fusion(bf16[256,2048]{1,0:T(8,128)(2,1)S(1)} %copy-done, bf16[72,2048]{1,0:T(8,128)(2,1)S(1)} %bitcast.37, bf16[2048,256]{1,0:T(8,128)(2,1)} %param.14, f32[72,256]{1,0:T(8,128)S(1)} %fusion.25), kind=kOutput, calls=%fused_computation.3 | convolution fusion | flops 151252992 | bytes 2760704 | tf_op jit(solution)/shard_map/dot_general | solution.py:71
  43.9 0.0 reduce-scatter.3.cloned.1.call-update
  43.9 0.0 reduce-scatter.5.cloned.1.call-start
  44.0 10.2 %all-gather.4.cloned.1.call-done = bf16[2048,256]{1,0:T(8,128)(2,1)} async-done(((bf16[256,256]{1,0:T(8,128)(2,1)}), bf16[2048,256]{1,0:T(8,128)(2,1)}) %all-gather.4.cloned.1.call-update) | async-done | bytes 1048592 | tf_op jit(solution)/shard_map/all_gather | solution.py:84
  54.2 1.5 fusion.26
  55.7 39.6 %all-gather.6.cloned.1.call-done = bf16[2048,256]{1,0:T(8,128)(2,1)} async-done(((bf16[256,256]{1,0:T(8,128)(2,1)}), bf16[2048,256]{1,0:T(8,128)(2,1)}) %all-gather.6.cloned.1.call-update) | async-done | bytes 1048592 | tf_op jit(solution)/shard_map/all_gather | solution.py:85
  95.3 40.2 %all-gather.8.cloned.1.call-done = bf16[256,2048]{1,0:T(8,128)(2,1)} async-done(((bf16[256,256]{1,0:T(8,128)(2,1)}), bf16[256,2048]{1,0:T(8,128)(2,1)}) %all-gather.8.cloned.1.call-update) | async-done | bytes 1048592 | tf_op jit(solution)/shard_map/all_gather | solution.py:92
  135.4 3.1 %convolution_convert_fusion.1 = bf16[64,2048]{1,0:T(8,128)(2,1)} fusion(bf16[256,2048]{1,0:T(8,128)(2,1)} %all-gather.8.cloned.1.call-done, bf16[64,2048]{1,0:T(8,128)(2,1)S(1)} %copy-done.1, bf16[2048,256]{1,0:T(8,128)(2,1)} %all-gather.6.cloned.1.call-done, f32[64,256]{1,0:T(8,128)S(1)} %fusion.26), kind=kOutput, calls=%fused_computation.2 | convolution fusion | flops 134447104 | bytes 2686976 | tf_op jit(solution)/shard_map/dot_general | solution.py:90
  138.5 0.0 reduce-scatter.5.cloned.1.call-update
  138.5 0.0 reduce-scatter.3.cloned.1.call-done
  138.6 1.7 %all_to_all.10 = bf16[1024,8,9]{0,2,1:T(8,128)(2,1)} reshape(bf16[1024,72]{0,1:T(8,128)(2,1)} %reduce-scatter.3.cloned.1.call-done) | data formatting | bytes 294912 | tf_op jit(solution)/shard_map/all_to_all | solution.py:78
  140.2 0.0 copy-start.3
  140.2 3.8 %all-to-all-start.1 = ((bf16[1024,8,9]{0,2,1:T(8,128)(2,1)}), bf16[1024,8,9]{0,2,1:T(8,128)(2,1)S(1)}, u32[]{:S(2)}, u32[]{:S(2)}) async-start(bf16[1024,8,9]{0,2,1:T(8,128)(2,1)} %all_to_all.10), calls=%async_computation.2 | async-start | bytes 524288 | tf_op jit(solution)/shard_map/all_to_all | solution.py:78
  144.0 0.0 copy-done.3
  144.0 8.2 %all-to-all-done.1 = bf16[1024,8,9]{0,2,1:T(8,128)(2,1)S(1)} async-done(((bf16[1024,8,9]{0,2,1:T(8,128)(2,1)}), bf16[1024,8,9]{0,2,1:T(8,128)(2,1)S(1)}, u32[]{:S(2)}, u32[]{:S(2)}) %all-to-all-start.1) | async-done | bytes 147488 | tf_op jit(solution)/shard_map/all_to_all | solution.py:78
  152.3 0.0 reduce-scatter.5.cloned.1.call-done
  152.3 0.0 copy-start.5
  152.3 0.6 copy-done.5
  153.0 2.0 %fusion.1 = bf16[64,1024]{1,0:T(8,128)(2,1)} fusion(f32[1024,9]{0,1:T(8,128)S(1)} %convert_reduce_fusion, bf16[64,1024]{1,0:T(8,128)(2,1)} %reduce-scatter.5.cloned.1.call-done, f32[1024]{0:T(1024)S(1)} %add_divide_fusion, f32[9]{0:T(128)S(1)} %bitcast.44, s32[9]{0:T(128)S(1)} %bitcast.43), kind=kOutput, calls=%fused_computation.5 | convolution fusion | flops 7341184 | bytes 303176 | tf_op jit(solution)/shard_map/fek,ekt->tf/dot_general | solution.py:82
  (11 shorter events, 0.2 us)
Async XLA Ops:
  7.4 33.8 %copy-start = (bf16[256,2048]{1,0:T(8,128)(2,1)S(1)}, bf16[256,2048]{1,0:T(8,128)(2,1)}, u32[]{:S(2)}) copy-start(bf16[256,2048]{1,0:T(8,128)(2,1)} %param.15) | copy-start | bytes 3145732
  7.4 2.3 %copy-start.1 = (bf16[64,2048]{1,0:T(8,128)(2,1)S(1)}, bf16[64,2048]{1,0:T(8,128)(2,1)}, u32[]{:S(2)}) copy-start(bf16[64,2048]{1,0:T(8,128)(2,1)} %param.10) | copy-start | bytes 786436
  7.4 46.8 %all-gather.4.cloned.1.call-start = ((), (), s32[]{:S(2)}) async-start(), calls=%async_computation.5 | async-start | bytes 1179648 | tf_op jit(solution)/shard_map/all_gather | solution.py:84
  8.1 87.2 %all-gather.6.cloned.1.call-start = ((), (), s32[]{:S(2)}) async-start(), calls=%async_computation.6 | async-start | bytes 1179648 | tf_op jit(solution)/shard_map/all_gather | solution.py:85
  8.8 0.8 copy-start.4
  8.9 126.6 %all-gather.8.cloned.1.call-start = ((), (), s32[]{:S(2)}) async-start(), calls=%async_computation.7 | async-start | bytes 1179648 | tf_op jit(solution)/shard_map/all_gather | solution.py:92
  9.6 129.0 %reduce-scatter.3.cloned.1.call-start = ((), (), s32[]{:S(2)}) async-start(), calls=%async_computation.4 | async-start | bytes 442368 | tf_op jit(solution)/shard_map/reduce_scatter | solution.py:70
  24.5 4.0 %collective-permute-start = (bf16[8,9,1,256]{3,0,2,1:T(8,128)(2,1)S(1)}, bf16[8,9,1,256]{3,0,2,1:T(8,128)(2,1)S(1)}, u32[]{:S(2)}, u32[]{:S(2)}) collective-permute-start(bf16[8,9,1,256]{3,0,2,1:T(8,128)(2,1)S(1)} %bitcast.41), channel_id=1, source_target_pairs={{0,2},{2,0},{4,6},{6,4},{8,10},{10,8},{12,14},{14,12},{1,3},{3,1},... | collective-permute-start | bytes 110600 | tf_op jit(solution)/shard_map/ppermute | solution.py:14
  28.5 4.9 %collective-permute-start.1 = (bf16[8,9,2,256]{3,0,2,1:T(8,128)(2,1)S(1)}, bf16[8,9,2,256]{3,0,2,1:T(8,128)(2,1)S(1)}, u32[]{:S(2)}, u32[]{:S(2)}) collective-permute-start(bf16[8,9,2,256]{3,0,2,1:T(8,128)(2,1)S(1)} %maximum_select_fusion.2), channel_id=1, source_target_pairs={{0,4},{4,0},{2,6},{6,2},{8,12},{12,8},{10,14},{14,10},{1,5},{5,1},... | collective-permute-start | bytes 221192 | tf_op jit(solution)/shard_map/ppermute | solution.py:14
  28.7 12.1 %copy-start.2 = (bf16[2048,256]{1,0:T(8,128)(2,1)S(1)}, bf16[2048,256]{1,0:T(8,128)(2,1)}, u32[]{:S(2)}) copy-start(bf16[2048,256]{1,0:T(8,128)(2,1)} %param.13) | copy-start | bytes 3145732
  33.5 7.2 %collective-permute-start.2 = (bf16[8,9,4,256]{3,0,2,1:T(8,128)(2,1)S(1)}, bf16[8,9,4,256]{3,0,2,1:T(8,128)(2,1)S(1)}, u32[]{:S(2)}, u32[]{:S(2)}) collective-permute-start(bf16[8,9,4,256]{3,0,2,1:T(8,128)(2,1)S(1)} %maximum_select_fusion.1), channel_id=1, source_target_pairs={{0,8},{8,0},{2,10},{10,2},{4,12},{12,4},{6,14},{14,6},{1,9},{9,1},... | collective-permute-start | bytes 442376 | tf_op jit(solution)/shard_map/ppermute | solution.py:14
  43.9 108.4 %reduce-scatter.5.cloned.1.call-start = ((), (), s32[]{:S(2)}) async-start(), calls=%async_computation.8 | async-start | bytes 393216 | tf_op jit(solution)/shard_map/reduce_scatter | solution.py:95
  140.2 3.8 %copy-start.3 = (f32[1024]{0:T(1024)S(1)}, f32[1024]{0:T(1024)}, u32[]{:S(2)}) copy-start(f32[1024]{0:T(1024)} %param.19) | copy-start | bytes 12292
  140.2 12.0 %all-to-all-start.1 = ((bf16[1024,8,9]{0,2,1:T(8,128)(2,1)}), bf16[1024,8,9]{0,2,1:T(8,128)(2,1)S(1)}, u32[]{:S(2)}, u32[]{:S(2)}) async-start(bf16[1024,8,9]{0,2,1:T(8,128)(2,1)} %all_to_all.10), calls=%async_computation.2 | async-start | bytes 524288 | tf_op jit(solution)/shard_map/all_to_all | solution.py:78
  152.3 0.7 copy-start.5
Sparse Core Ops, SparseCore 0:
  10.3 43.8 all-gather.3
  56.3 38.9 all-gather.5
  97.3 38.0 all-gather.7
Sparse Core Ops, SparseCore 1:
  44.0 5.7 reduce-scatter.2
  138.6 6.7 reduce-scatter.4
where the time goes:
time: 163 us; the launch traced here: 162 us
  waiting for transfers between devices  115 us (71%)
  between operations  14.7 us (9%)
  blocking collectives  14.1 us (9%)
  matrix products  9.66 us (6%)
  starting transfers between devices  4.97 us (3%)
  local copies, waits for them, and re-layouts  3.09 us (2%)
    all_gather x1, waiting for transfers between devices, local(): lax.all_gather(dense_down, 'ep', axis=1, tiled=True)  40.2 us
    all_gather x1, waiting for transfers between devices, local(): lax.all_gather(dense_up, 'ep', axis=0, tiled=True)  39.6 us
    ppermute x3, waiting for transfers between devices, swapped(): return lax.ppermute(block, axis, route)  15.1 us
    all_to_all x1, blocking collectives, local(): lax.all_to_all(split_rows, 'ep', split_axis=0, concat_axis=0, tiled=True)  14.1 us
    all_gather x1, waiting for transfers between devices, local(): lax.all_gather(dense_gate, 'ep', axis=0, tiled=True)  10.2 us
    all_to_all x1, waiting for transfers between devices, local(): lax.all_to_all(member_sums, 'ep', split_axis=1, concat_axis=1, tiled=True)  8.21 us
    all_to_all x1, starting transfers between devices, local(): lax.all_to_all(member_sums, 'ep', split_axis=1, concat_axis=1, tiled=True)  3.76 us
  transfers between devices with their start and end apart: 9, of which 7 were waited for; matrix products, arithmetic and copies ran while one was open for 5% of the time, Pallas kernels for 0%

commit v1 on v0

--- a/solution.py
+++ b/solution.py
@@ -2,6 +2,13 @@
 import jax.numpy as jnp
 from jax import lax
 from jax.sharding import PartitionSpec as P
+
+
+def trade_parts(value, name, split, join):
+    count = lax.axis_size(name)
+    blocks = jnp.stack(jnp.split(value, count, axis=split), axis=0)
+    blocks = lax.all_to_all(blocks, name, split_axis=0, concat_axis=0)
+    return jnp.concatenate(blocks, axis=join)
 
 
 def swapped(block, axis, apart):
@@ -75,7 +82,7 @@
         scatter_dimension=0,
         tiled=True,
     )
-    returned = lax.all_to_all(member_sums, "ep", split_axis=1, concat_axis=1, tiled=True)
+    returned = trade_parts(member_sums, "ep", 1, 1)
     summed = returned.astype(jnp.float32).reshape(width // 2, experts, 8, slots).sum(axis=2)
     positions = lax.broadcasted_iota(jnp.int32, (experts, slots, tok_local), 2)
     weights_table = jnp.where(picked[:, :, None] == positions, route_weight[:, 0, :, None], 0.0)

time: 163 us -> 193 us (1.18)
  waiting for transfers between devices: 115 us -> 134 us
  local copies, waits for them, and re-layouts: 3.09 us -> 15.2 us
    all_gather x1, waiting for transfers between devices: 10.2 us -> 25.1 us  [local(): lax.all_gather(dense_gate, 'ep', axis=0, tiled=True)]
    unnamed x14 -> x23, local copies, waits for them, and re-layouts: 0.74 us -> 12.1 us
    reduce_scatter x1, waiting for transfers between devices: 0.03 us -> 4.29 us  [local(): lax.psum_scatter(lax.dot_general(shard_rows, flat_hidden, (((0,), (1,)),...]
  transfers between devices with their start and end apart: 9 -> 9, of which waited for: 7 -> 8; matrix products, arithmetic and copies ran while one was open for 5% -> 7% of each run, Pallas kernels for 0% -> 0%
where the time goes in v1:
time: 193 us; the launch traced here: 192 us
  waiting for transfers between devices  134 us (69%)
  local copies, waits for them, and re-layouts  15.2 us (8%)
  between operations  15.2 us (8%)
  blocking collectives  14 us (7%)
  matrix products  8.4 us (4%)
  starting transfers between devices  5.5 us (3%)
    all_gather x1, waiting for transfers between devices, local(): lax.all_gather(dense_down, 'ep', axis=1, tiled=True)  39.9 us
    all_gather x1, waiting for transfers between devices, local(): lax.all_gather(dense_up, 'ep', axis=0, tiled=True)  39.5 us
    all_gather x1, waiting for transfers between devices, local(): lax.all_gather(dense_gate, 'ep', axis=0, tiled=True)  25.1 us
    ppermute x3, waiting for transfers between devices, swapped(): return lax.ppermute(block, axis, route)  15 us
    all_to_all x1, blocking collectives, local(): lax.all_to_all(split_rows, 'ep', split_axis=0, concat_axis=0, tiled=True)  14 us
    unnamed x23, local copies, waits for them, and re-layouts  12.1 us
    all_to_all x1, waiting for transfers between devices, trade_parts(): blocks = lax.all_to_all(blocks, name, split_axis=0, concat_axis=0)  8.2 us
    reduce_scatter x1, waiting for transfers between devices, local(): lax.psum_scatter(lax.dot_general(shard_rows, flat_hidden, (((0,), (1,)),...  4.29 us
  transfers between devices with their start and end apart: 9, of which 8 were waited for; matrix products, arithmetic and copies ran while one was open for 7% of the time, Pallas kernels for 0%

profile of v1, /device:TPU:0, one launch (start us, length us, event | category | flops | bytes accessed | tf_op | source)
XLA Modules:
  0.0 192.0 jit_solution(7165722620833087204)
XLA Ops:
  7.4 0.0 copy-start
  7.4 0.0 copy-start.5
  7.4 0.0 reduce-scatter.3.cloned.1.call-start
  7.4 0.7 copy-done.5
  8.1 1.6 gather_fusion
  9.8 0.1 fusion.10
  9.9 14.0 %all_to_all.10 = bf16[8,9,256]{2,1,0:T(8,128)(2,1)S(1)} all-to-all(bf16[8,9,256]{2,1,0:T(8,128)(2,1)S(1)} %fusion.10), channel_id=1, replica_groups=mesh['grp'=2,'ep'=8,'tp'=2] {'ep'}, dimensions={0} | all-to-all | bytes 73728 | tf_op jit(solution)/shard_map/all_to_all | solution.py:64
  23.9 0.5 collective-permute-start
  24.3 3.6 %collective-permute-done = bf16[8,9,1,256]{3,0,2,1:T(8,128)(2,1)S(1)} collective-permute-done((bf16[8,9,1,256]{3,0,2,1:T(8,128)(2,1)S(1)}, bf16[8,9,1,256]{3,0,2,1:T(8,128)(2,1)S(1)}, u32[]{:S(2)}, u32[]{:S(2)}) %collective-permute-start) | collective-permute-done | bytes 36896 | tf_op jit(solution)/shard_map/ppermute | solution.py:21
  27.9 0.3 collective-permute-start.1
  28.2 0.0 copy-start.2
  28.2 4.4 %collective-permute-done.1 = bf16[8,9,2,256]{3,0,2,1:T(8,128)(2,1)S(1)} collective-permute-done((bf16[8,9,2,256]{3,0,2,1:T(8,128)(2,1)S(1)}, bf16[8,9,2,256]{3,0,2,1:T(8,128)(2,1)S(1)}, u32[]{:S(2)}, u32[]{:S(2)}) %collective-permute-start.1) | collective-permute-done | bytes 73760 | tf_op jit(solution)/shard_map/ppermute | solution.py:21
  32.7 0.7 collective-permute-start.2
  33.4 6.9 %collective-permute-done.2 = bf16[8,9,4,256]{3,0,2,1:T(8,128)(2,1)S(1)} collective-permute-done((bf16[8,9,4,256]{3,0,2,1:T(8,128)(2,1)S(1)}, bf16[8,9,4,256]{3,0,2,1:T(8,128)(2,1)S(1)}, u32[]{:S(2)}, u32[]{:S(2)}) %collective-permute-start.2) | collective-permute-done | bytes 147488 | tf_op jit(solution)/shard_map/ppermute | solution.py:21
  40.4 0.1 copy.15
  40.4 0.0 copy-start.3
  40.4 0.1 copy.17
  40.5 0.0 copy-done.2
  40.5 0.3 fusion.33
  40.8 0.0 copy-done
  40.8 0.8 copy-done.3
  41.7 1.5 fusion
  43.1 0.0 reduce-scatter.3.cloned.1.call-update
  43.2 0.0 all-gather.4.cloned.1.call-start
  43.2 0.5 all-gather.4.cloned.1.call-update
  43.7 0.0 all-gather.6.cloned.1.call-start
  43.8 0.5 all-gather.6.cloned.1.call-update
  44.3 0.0 all-gather.8.cloned.1.call-start
  44.4 0.5 all-gather.8.cloned.1.call-update
  44.9 0.0 copy-start.1
  44.9 0.0 reduce-scatter.5.cloned.1.call-start
  45.0 4.3 %reduce-scatter.3.cloned.1.call-done = bf16[1024,72]{0,1:T(8,128)(2,1)} async-done(((bf16[2048,72]{0,1:T(8,128)(2,1)}), bf16[1024,72]{0,1:T(8,128)(2,1)}) %reduce-scatter.3.cloned.1.call-update) | async-done | bytes 147472 | tf_op jit(solution)/shard_map/reduce_scatter | solution.py:77
  49.3 1.4 fusion.24
  50.6 1.4 fusion.23
  52.0 1.4 fusion.22
  53.4 1.4 fusion.21
  54.9 1.4 fusion.20
  56.3 1.4 fusion.19
  57.7 1.4 fusion.18
  59.1 25.1 %all-gather.4.cloned.1.call-done = bf16[2048,256]{1,0:T(8,128)(2,1)} async-done(((bf16[256,256]{1,0:T(8,128)(2,1)}), bf16[2048,256]{1,0:T(8,128)(2,1)}) %all-gather.4.cloned.1.call-update) | async-done | bytes 1048592 | tf_op jit(solution)/shard_map/all_gather | solution.py:91
  84.2 0.0 copy-done.1
  84.2 1.5 fusion.34
  85.7 39.5 %all-gather.6.cloned.1.call-done = bf16[2048,256]{1,0:T(8,128)(2,1)} async-done(((bf16[256,256]{1,0:T(8,128)(2,1)}), bf16[2048,256]{1,0:T(8,128)(2,1)}) %all-gather.6.cloned.1.call-update) | async-done | bytes 1048592 | tf_op jit(solution)/shard_map/all_gather | solution.py:92
  125.2 39.9 %all-gather.8.cloned.1.call-done = bf16[256,2048]{1,0:T(8,128)(2,1)} async-done(((bf16[256,256]{1,0:T(8,128)(2,1)}), bf16[256,2048]{1,0:T(8,128)(2,1)}) %all-gather.8.cloned.1.call-update) | async-done | bytes 1048592 | tf_op jit(solution)/shard_map/all_gather | solution.py:99
  165.1 3.0 %convolution_convert_fusion.1 = bf16[64,2048]{1,0:T(8,128)(2,1)} fusion(bf16[256,2048]{1,0:T(8,128)(2,1)} %all-gather.8.cloned.1.call-done, bf16[64,2048]{1,0:T(8,128)(2,1)S(1)} %copy-done.1, bf16[2048,256]{1,0:T(8,128)(2,1)} %all-gather.6.cloned.1.call-done, f32[64,256]{1,0:T(8,128)S(1)} %fusion.34), kind=kOutput, calls=%fused_computation.2 | convolution fusion | flops 134447104 | bytes 2686976 | tf_op jit(solution)/shard_map/dot_general | solution.py:97
  168.2 0.0 reduce-scatter.5.cloned.1.call-update
  168.2 1.4 fusion.17
  169.6 0.0 copy-start.4
  169.6 3.9 %all-to-all-start.1 = ((bf16[8,1024,9]{1,2,0:T(8,128)(2,1)}), bf16[8,1024,9]{1,2,0:T(8,128)(2,1)S(1)}, u32[]{:S(2)}, u32[]{:S(2)}) async-start(bf16[8,1024,9]{1,2,0:T(8,128)(2,1)} %fusion.17), calls=%async_computation.2 | async-start | bytes 524288 | tf_op jit(solution)/shard_map/all_to_all | solution.py:10
  173.4 0.0 copy-done.4
  173.5 8.2 %all-to-all-done.1 = bf16[8,1024,9]{1,2,0:T(8,128)(2,1)S(1)} async-done(((bf16[8,1024,9]{1,2,0:T(8,128)(2,1)}), bf16[8,1024,9]{1,2,0:T(8,128)(2,1)S(1)}, u32[]{:S(2)}, u32[]{:S(2)}) %all-to-all-start.1) | async-done | bytes 147488 | tf_op jit(solution)/shard_map/all_to_all | solution.py:10
  181.7 0.0 reduce-scatter.5.cloned.1.call-done
  181.7 0.0 copy-start.6
  181.8 0.6 copy-done.6
  182.4 2.1 %fusion.1 = bf16[64,1024]{1,0:T(8,128)(2,1)} fusion(f32[1024,9]{0,1:T(8,128)S(1)} %convert_reduce_fusion, bf16[64,1024]{1,0:T(8,128)(2,1)} %reduce-scatter.5.cloned.1.call-done, f32[1024]{0:T(1024)S(1)} %add_divide_fusion, f32[9]{0:T(128)S(1)} %bitcast.74, s32[9]{0:T(128)S(1)} %bitcast.73), kind=kOutput, calls=%fused_computation.5 | convolution fusion | flops 7341184 | bytes 303176 | tf_op jit(solution)/shard_map/fek,ekt->tf/dot_general | solution.py:89
  (11 shorter events, 0.2 us)
Async XLA Ops:
  7.4 33.5 %copy-start = (bf16[256,2048]{1,0:T(8,128)(2,1)S(1)}, bf16[256,2048]{1,0:T(8,128)(2,1)}, u32[]{:S(2)}) copy-start(bf16[256,2048]{1,0:T(8,128)(2,1)} %param.15) | copy-start | bytes 3145732
  7.4 0.7 copy-start.5
  7.4 41.9 %reduce-scatter.3.cloned.1.call-start = ((), (), s32[]{:S(2)}) async-start(), calls=%async_computation.4 | async-start | bytes 442368 | tf_op jit(solution)/shard_map/reduce_scatter | solution.py:77
  23.9 4.0 %collective-permute-start = (bf16[8,9,1,256]{3,0,2,1:T(8,128)(2,1)S(1)}, bf16[8,9,1,256]{3,0,2,1:T(8,128)(2,1)S(1)}, u32[]{:S(2)}, u32[]{:S(2)}) collective-permute-start(bf16[8,9,1,256]{3,0,2,1:T(8,128)(2,1)S(1)} %bitcast.71), channel_id=1, source_target_pairs={{0,2},{2,0},{4,6},{6,4},{8,10},{10,8},{12,14},{14,12},{1,3},{3,1},... | collective-permute-start | bytes 110600 | tf_op jit(solution)/shard_map/ppermute | solution.py:21
  27.9 4.7 %collective-permute-start.1 = (bf16[8,9,2,256]{3,0,2,1:T(8,128)(2,1)S(1)}, bf16[8,9,2,256]{3,0,2,1:T(8,128)(2,1)S(1)}, u32[]{:S(2)}, u32[]{:S(2)}) collective-permute-start(bf16[8,9,2,256]{3,0,2,1:T(8,128)(2,1)S(1)} %maximum_select_fusion.2), channel_id=1, source_target_pairs={{0,4},{4,0},{2,6},{6,2},{8,12},{12,8},{10,14},{14,10},{1,5},{5,1},... | collective-permute-start | bytes 221192 | tf_op jit(solution)/shard_map/ppermute | solution.py:21
  28.2 12.3 %copy-start.2 = (bf16[2048,256]{1,0:T(8,128)(2,1)S(1)}, bf16[2048,256]{1,0:T(8,128)(2,1)}, u32[]{:S(2)}) copy-start(bf16[2048,256]{1,0:T(8,128)(2,1)} %param.13) | copy-start | bytes 3145732
  32.7 7.7 %collective-permute-start.2 = (bf16[8,9,4,256]{3,0,2,1:T(8,128)(2,1)S(1)}, bf16[8,9,4,256]{3,0,2,1:T(8,128)(2,1)S(1)}, u32[]{:S(2)}, u32[]{:S(2)}) collective-permute-start(bf16[8,9,4,256]{3,0,2,1:T(8,128)(2,1)S(1)} %maximum_select_fusion.1), channel_id=1, source_target_pairs={{0,8},{8,0},{2,10},{10,2},{4,12},{12,4},{6,14},{14,6},{1,9},{9,1},... | collective-permute-start | bytes 442376 | tf_op jit(solution)/shard_map/ppermute | solution.py:21
  40.4 1.2 copy-start.3
  43.2 41.0 %all-gather.4.cloned.1.call-start = ((), (), s32[]{:S(2)}) async-start(), calls=%async_computation.5 | async-start | bytes 1179648 | tf_op jit(solution)/shard_map/all_gather | solution.py:91
  43.7 81.5 %all-gather.6.cloned.1.call-start = ((), (), s32[]{:S(2)}) async-start(), calls=%async_computation.6 | async-start | bytes 1179648 | tf_op jit(solution)/shard_map/all_gather | solution.py:92
  44.3 120.8 %all-gather.8.cloned.1.call-start = ((), (), s32[]{:S(2)}) async-start(), calls=%async_computation.7 | async-start | bytes 1179648 | tf_op jit(solution)/shard_map/all_gather | solution.py:99
  44.9 39.3 %copy-start.1 = (bf16[64,2048]{1,0:T(8,128)(2,1)S(1)}, bf16[64,2048]{1,0:T(8,128)(2,1)}, u32[]{:S(2)}) copy-start(bf16[64,2048]{1,0:T(8,128)(2,1)} %param.10) | copy-start | bytes 786436
  44.9 136.8 %reduce-scatter.5.cloned.1.call-start = ((), (), s32[]{:S(2)}) async-start(), calls=%async_computation.8 | async-start | bytes 393216 | tf_op jit(solution)/shard_map/reduce_scatter | solution.py:102
  169.6 3.9 %copy-start.4 = (f32[1024]{0:T(1024)S(1)}, f32[1024]{0:T(1024)}, u32[]{:S(2)}) copy-start(f32[1024]{0:T(1024)} %param.19) | copy-start | bytes 12292
  169.6 12.1 %all-to-all-start.1 = ((bf16[8,1024,9]{1,2,0:T(8,128)(2,1)}), bf16[8,1024,9]{1,2,0:T(8,128)(2,1)S(1)}, u32[]{:S(2)}, u32[]{:S(2)}) async-start(bf16[8,1024,9]{1,2,0:T(8,128)(2,1)} %fusion.17), calls=%async_computation.2 | async-start | bytes 524288 | tf_op jit(solution)/shard_map/all_to_all | solution.py:10
  181.7 0.7 copy-start.6
Sparse Core Ops, SparseCore 0:
  43.3 5.9 reduce-scatter.2
  168.3 6.8 reduce-scatter.4
Sparse Core Ops, SparseCore 1:
  45.8 38.4 all-gather.3
  86.2 38.9 all-gather.5
  127.1 38.0 all-gather.7
